TPU v7x, 32 devices: a whole 2x2x4 slice. The times are simulated.
32 devices in a mesh: ep: 8 (over z, y), tp: 4 (over x, core).
Axes of the slice: x: 2, y: 2, z: 4, core: 2. Of those that a mesh axis runs over, the one named last changes fastest.
Arguments:
- conv_value: bfloat16 [3072, 2048], P('ep', 'tp'), may hold values from -36 to 36
- conv_gate: bfloat16 [3072, 2048], P('ep', 'tp'), may hold values from -8 to 8
- conv_taps: bfloat16 [31, 2048], P(None, 'tp'), may hold values from -1 to 1
- conv_gain: float32 [2048], P('tp'), may hold values from 0.1 to 1.9
- conv_proj: bfloat16 [2048, 2048], P('tp'), may hold values from -0.125 to 0.125
- moe_tokens: bfloat16 [3072, 2048], P('ep'), may hold values from -6 to 6
- moe_gain: float32 [2048], replicated, may hold values from 0.1 to 1.9
- routes: int32 [3072, 2], P('ep'), may hold values from 0 to 7, all different within a row; in each aligned block of 384 rows (0 to 383, 384 to 767, ...) at most 144 rows name the same one
- route_weights: float32 [3072, 2], P('ep'), may hold values from 0.3 to 3
- expert_gate: bfloat16 [8, 2048, 1024], P('ep', None, 'tp'), may hold values from -0.125 to 0.125
- expert_up: bfloat16 [8, 2048, 1024], P('ep', None, 'tp'), may hold values from -0.125 to 0.125
- expert_down: bfloat16 [8, 1024, 2048], P('ep', 'tp'), may hold values from -0.1875 to 0.1875
- shared_gate: bfloat16 [2048, 256], replicated, may hold values from -0.125 to 0.125
- shared_up: bfloat16 [2048, 256], replicated, may hold values from -0.125 to 0.125
- shared_down: bfloat16 [256, 2048], P(None, 'tp'), may hold values from -0.375 to 0.375
Outputs:
- conv_result: bfloat16 [3072, 2048], P('ep', 'tp')
- moe_result: bfloat16 [3072, 2048], P('ep', 'tp')
Inputs may be any that keep to these rules, and one draw needn't show every extreme that they name: `routes`: each row names 2 different experts. Among the 384 rows of one index of ep (aligned blocks in order) no expert is named more than 144 times, and in some blocks one expert is named exactly 144 times.
All inputs are finite; a program needn't handle non-finite values.
Results may differ from a plain program's by a relative error of at most 0.01.
Values may be sent and summed in bfloat16 or wider, within the bound.
A program may use at most 64 MiB of HBM per device.

v0:
```python
import jax
import jax.numpy as jnp
from jax import lax
from jax.sharding import PartitionSpec as P

epsilon = 1e-05


def passed_along(value, axis, by):
    devices = lax.axis_size(axis)
    pairs = [(i, i + by) for i in range(devices) if 0 <= i + by < devices]
    return lax.ppermute(value, axis, pairs)


def shared_hidden_rows(rows, shared_gate, shared_up):
    return (
        jax.nn.silu(jnp.dot(rows, shared_gate, preferred_element_type=jnp.float32))
        * jnp.dot(rows, shared_up, preferred_element_type=jnp.float32)
    ).astype(jnp.bfloat16)


def local(
    conv_value,
    conv_gate,
    conv_taps,
    conv_gain,
    conv_proj,
    moe_tokens,
    moe_gain,
    routes,
    route_weights,
    expert_gate,
    expert_up,
    expert_down,
    shared_gate,
    shared_up,
    shared_down,
):
    model_width = moe_tokens.shape[1]
    tok_rows = conv_value.shape[0]
    kernel = conv_taps.shape[0]
    gated_rows = (
        conv_value.astype(jnp.float32) * jax.nn.sigmoid(conv_gate.astype(jnp.float32))
    ).astype(jnp.bfloat16)
    previous = passed_along(gated_rows[tok_rows - (kernel - 1) :], "ep", 1)
    padded = jnp.concatenate([previous, gated_rows], axis=0).astype(jnp.float32)
    tap_weights = conv_taps.astype(jnp.float32)
    convolved = jnp.zeros(gated_rows.shape, jnp.float32)
    for offset in range(kernel):
        convolved = convolved + tap_weights[offset][None, :] * padded[offset : offset + tok_rows]
    total_sum, square_sum = lax.psum(
        (jnp.sum(convolved, axis=1), jnp.sum(convolved * convolved, axis=1)), "tp"
    )
    average = total_sum / model_width
    variance = square_sum / model_width - average * average
    scaled = (
        (convolved - average[:, None]) * lax.rsqrt(variance + epsilon)[:, None] * conv_gain[None, :]
    )
    activated = jax.nn.silu(scaled).astype(jnp.bfloat16)
    conv_partial = jnp.dot(activated, conv_proj, preferred_element_type=jnp.float32)
    tokens = moe_tokens.astype(jnp.float32)
    token_mean = jnp.mean(tokens, axis=1, keepdims=True)
    centered = tokens - token_mean
    token_var = jnp.mean(centered * centered, axis=1, keepdims=True)
    normalized = (centered * lax.rsqrt(token_var + epsilon) * moe_gain[None, :]).astype(
        jnp.bfloat16
    )
    shared_hidden = shared_hidden_rows(normalized, shared_gate, shared_up)
    shared_part = jnp.dot(shared_hidden, shared_down, preferred_element_type=jnp.float32)
    experts = lax.axis_size("ep")
    top_count = routes.shape[1]
    capacity = 3 * tok_rows * top_count // (2 * experts)
    entries = tok_rows * top_count
    flat_routes = routes.reshape(-1)
    one_hot = (flat_routes[:, None] == jnp.arange(experts, dtype=jnp.int32)[None, :]).astype(
        jnp.int32
    )
    before = jnp.cumsum(one_hot, axis=0) - one_hot
    slot_rank = jnp.sum(before * one_hot, axis=1)
    slot_index = flat_routes * capacity + slot_rank
    source_row = (
        jnp.full((experts * capacity,), -1, jnp.int32)
        .at[slot_index]
        .set(jnp.arange(entries, dtype=jnp.int32))
    )
    filled = source_row >= 0
    token_index = jnp.where(filled, source_row // top_count, 0)
    outgoing = jnp.where(filled[:, None], normalized[token_index], jnp.zeros((), jnp.bfloat16))
    outgoing = outgoing.reshape(experts, capacity, model_width)
    quarter = model_width // lax.axis_size("tp")
    first_column = lax.axis_index("tp") * quarter
    column_block = lax.dynamic_slice_in_dim(outgoing, first_column, quarter, 2)
    arrived = lax.all_to_all(column_block, "ep", split_axis=0, concat_axis=0, tiled=True)
    arrived = lax.all_gather(arrived, "tp", axis=2, tiled=True)
    expert_input = arrived.reshape(experts * capacity, model_width)
    hidden = (
        jax.nn.silu(jnp.dot(expert_input, expert_gate[0], preferred_element_type=jnp.float32))
        * jnp.dot(expert_input, expert_up[0], preferred_element_type=jnp.float32)
    ).astype(jnp.bfloat16)
    expert_partial = jnp.dot(hidden, expert_down[0], preferred_element_type=jnp.float32)
    conv_sum, expert_sum = (
        lax.psum_scatter(
            conv_partial.astype(jnp.bfloat16), "tp", scatter_dimension=1, tiled=True
        ).astype(jnp.float32),
        lax.psum_scatter(
            expert_partial.astype(jnp.bfloat16), "tp", scatter_dimension=1, tiled=True
        ).astype(jnp.float32),
    )
    conv_result = conv_sum.astype(jnp.bfloat16)
    expert_rows = expert_sum.astype(jnp.bfloat16).reshape(experts, capacity, expert_sum.shape[1])
    returned = lax.all_to_all(expert_rows, "ep", split_axis=0, concat_axis=0, tiled=True)
    picked = returned.reshape(experts * capacity, returned.shape[2])[slot_index]
    picked = picked.astype(jnp.float32).reshape(tok_rows, top_count, returned.shape[2])
    moe_result = (shared_part + jnp.sum(route_weights[:, :, None] * picked, axis=1)).astype(
        jnp.bfloat16
    )
    return (conv_result, moe_result)


def solution(mesh):
    placed = (
        P("ep", "tp"),
        P("ep", "tp"),
        P(None, "tp"),
        P("tp"),
        P("tp", None),
        P("ep", None),
        P(),
        P("ep", None),
        P("ep", None),
        P("ep", None, "tp"),
        P("ep", None, "tp"),
        P("ep", "tp", None),
        P(),
        P(),
        P(None, "tp"),
    )
    return jax.shard_map(
        local, mesh=mesh, in_specs=placed, out_specs=(P("ep", "tp"), P("ep", "tp")), check_vma=False
    )
```

profile of v0, /device:TPU:0, one launch (start us, length us, event | category | flops | bytes accessed | tf_op | source)
XLA Modules:
  0.0 224.0 jit_solution(10507383966461144714)
XLA Ops:
  7.2 1.0 copy.22
  8.2 0.1 eq.29
  8.3 0.1 eq.25
  8.5 0.7 broadcast_multiply_fusion
  9.2 1.7 reduce-window.6
  11.1 0.2 reduce-window.9
  11.5 0.2 mul.513
  11.8 3.4 %scatter_custom_fusion = s32[1152]{0:T(1024)S(1)} fusion(s32[768]{0:T(1024)S(1)} %fusion.67, s32[768]{0:T(1024)S(1)} %iota.11, s32[]{:T(128)} %constant.26.clone.1), kind=kCustom, calls=%fused_computation.124 | custom fusion | bytes 4612 | tf_op jit(solution)/shard_map/scatter | solution.py:84
  15.2 1.8 convert_reduce_fusion
  17.1 0.6 fusion.2
  17.7 3.1 %fusion.4 = bf16[384,2048]{1,0:T(8,128)(2,1)} fusion(bf16[384,2048]{1,0:T(8,128)(2,1)} %param.20, f32[2048]{0:T(1024)S(1)} %copy-done.5, f32[384]{0:T(512)S(1)} %add_rsqrt_fusion, f32[384]{0:T(512)S(1)} %broadcast_multiply_fusion.1), kind=kLoop, calls=%fused_computation.10 | loop fusion | flops 3932160 | bytes 3156992 | tf_op jit(solution)/shard_map/convert_element_type | solution.py:65
  20.9 12.3 %gather_fusion = bf16[1152,2048]{1,0:T(8,128)(2,1)} fusion(bf16[384,2048]{1,0:T(8,128)(2,1)} %fusion.4, s32[2048]{0:T(1024)S(1)} %pad_clamp_fusion), kind=kCustom, calls=%fused_computation | custom fusion | bytes 9441792 | tf_op jit(solution)/shard_map/gather | solution.py:88
  33.1 1.6 dynamic-slice_select_fusion
  34.7 36.2 %all_to_all.10 = bf16[8,144,512]{2,1,0:T(8,128)(2,1)} all-to-all(bf16[8,144,512]{2,1,0:T(8,128)(2,1)S(1)} %dynamic-slice_select_fusion), channel_id=1, replica_groups=mesh['ep'=8,'tp'=4] {'ep'}, dimensions={0} | all-to-all | bytes 2359296 | tf_op jit(solution)/shard_map/all_to_all | solution.py:93
  71.1 36.2 %all-gather.2.cloned.1.call-done = bf16[8,144,2048]{2,1,0:T(8,128)(2,1)} async-done(((bf16[8,144,512]{2,1,0:T(8,128)(2,1)}), bf16[8,144,2048]{2,1,0:T(8,128)(2,1)}) %all-gather.2.cloned.1.call-update) | async-done | bytes 4718608 | tf_op jit(solution)/shard_map/all_gather | solution.py:94
  107.3 4.7 %fusion.16 = f32[1152,256]{1,0:T(8,128)} fusion(bf16[1152,2048]{1,0:T(8,128)(2,1)} %bitcast.99, bf16[1,2048,256]{2,1,0:T(8,128)(2,1)S(1)} %copy-done.7), kind=kOutput, calls=%fused_computation.27 | convolution fusion | flops 1207959552 | bytes 6946816 | tf_op jit(solution)/shard_map/dot_general | solution.py:97
  112.0 10.3 %convolution_convert_fusion = bf16[1152,2048]{1,0:T(8,128)(2,1)} fusion(bf16[1152,2048]{1,0:T(8,128)(2,1)} %bitcast.100, f32[1152,256]{1,0:T(8,128)} %fusion.16, bf16[1,256,2048]{2,1,0:T(8,128)(2,1)} %param.26, bf16[1,2048,256]{2,1,0:T(8,128)(2,1)} %param.25), kind=kOutput, calls=%fused_computation.3 | convolution fusion | flops 2420047872 | bytes 12713984 | tf_op jit(solution)/shard_map/dot_general | solution.py:100
  122.4 0.9 copy-done.2
  123.4 0.2 multiply_convert_fusion.1
  123.6 3.6 %collective-permute-start = (bf16[30,512]{1,0:T(8,128)(2,1)S(1)}, bf16[30,512]{1,0:T(8,128)(2,1)S(1)}, u32[]{:S(2)}, u32[]{:S(2)}) collective-permute-start(bf16[30,512]{1,0:T(8,128)(2,1)S(1)} %slice.265), channel_id=1, source_target_pairs={{0,4},{4,8},{8,12},{12,16},{16,20},{20,24},{24,28},{1,5},{5,9},{9,... | collective-permute-start | bytes 92168 | tf_op jit(solution)/shard_map/ppermute | solution.py:12
  127.3 1.3 collective-permute-done
  128.7 3.8 %fusion.71 = (f32[384]{0:T(512)S(1)}, f32[384]{0:T(512)S(1)}, f32[384,512]{1,0:T(8,128)S(1)}) fusion(f32[414,512]{1,0:T(8,128)S(1)} %maximum_convert_fusion, f32[512]{0:T(512)S(1)} %bitcast.98, f32[512]{0:T(512)S(1)} %bitcast.97, f32[512]{0:T(512)S(1)} %bitcast.96, f32[512]{0:T(512)S(1)} %bitcast.95, f32[512]{0:T(512)S(1)} %bitcast.94, f32[512]{0:T(512)S(1)} %bitcast.93, ...), kind=kLoop, calls=%fused_computation.135 | loop fusion | flops 12582144 | bytes 25232384 | tf_op jit(solution)/shard_map/reduce_sum | solution.py:52
  132.6 6.0 %all-reduce = (f32[384]{0:T(512)S(1)}, f32[384]{0:T(512)S(1)}) all-reduce(f32[384]{0:T(512)S(1)} %get-tuple-element.3, f32[384]{0:T(512)S(1)} %get-tuple-element.2), channel_id=1, replica_groups=mesh['ep'=8,'tp'=4] {'tp'}, use_global_device_ids=true, to_apply=%region_3.0 | all-reduce | flops 768 | bytes 6144 | tf_op jit(solution)/shard_map/psum | solution.py:51
  138.6 2.3 %convolution_convert_fusion.1 = bf16[384,2048]{1,0:T(8,128)(2,1)} fusion(bf16[512,2048]{1,0:T(8,128)(2,1)S(1)} %copy-done, f32[384,512]{1,0:T(8,128)S(1)} %get-tuple-element.6, f32[512]{0:T(512)S(1)} %copy-done.9, f32[384]{0:T(512)S(1)} %get-tuple-element.39, f32[384]{0:T(512)S(1)} %get-tuple-element.38), kind=kOutput, calls=%fused_computation.12 | convolution fusion | flops 807665664 | bytes 4461568 | tf_op jit(solution)/shard_map/dot_general | solution.py:60
  140.9 29.3 %reduce-scatter.5.cloned.1.call-done = bf16[1152,512]{1,0:T(8,128)(2,1)} async-done(((bf16[1152,2048]{1,0:T(8,128)(2,1)}), bf16[1152,512]{1,0:T(8,128)(2,1)}) %reduce-scatter.5.cloned.1.call-update) | async-done | bytes 1179664 | tf_op jit(solution)/shard_map/reduce_scatter | solution.py:105
  170.3 5.5 %all-to-all-start.1 = ((bf16[8,144,512]{2,1,0:T(8,128)(2,1)}), bf16[8,144,512]{2,1,0:T(8,128)(2,1)S(1)}, u32[]{:S(2)}, u32[]{:S(2)}) async-start(bf16[8,144,512]{2,1,0:T(8,128)(2,1)} %bitcast.65), calls=%async_computation.3 | async-start | bytes 2359296 | tf_op jit(solution)/shard_map/all_to_all | solution.py:111
  175.9 3.0 %fusion.75 = f32[384,256]{1,0:T(8,128)} fusion(bf16[384,2048]{1,0:T(8,128)(2,1)} %fusion.4, bf16[2048,256]{1,0:T(8,128)(2,1)} %param.27), kind=kOutput, calls=%fused_computation.138 | convolution fusion | flops 402653184 | bytes 3014656 | tf_op jit(solution)/shard_map/dot_general | solution.py:17
  179.0 25.2 %all-to-all-done.1 = bf16[8,144,512]{2,1,0:T(8,128)(2,1)S(1)} async-done(((bf16[8,144,512]{2,1,0:T(8,128)(2,1)}), bf16[8,144,512]{2,1,0:T(8,128)(2,1)S(1)}, u32[]{:S(2)}, u32[]{:S(2)}) %all-to-all-start.1) | async-done | bytes 1179680 | tf_op jit(solution)/shard_map/all_to_all | solution.py:111
  204.2 3.3 %gather_fusion.1 = bf16[768,512]{1,0:T(8,128)(2,1)} fusion(bf16[1152,512]{1,0:T(8,128)(2,1)S(1)} %bitcast.63, s32[1024]{0:T(1024)S(1)} %pad_clamp_fusion.1), kind=kCustom, calls=%fused_computation.1 | custom fusion | bytes 1575936 | tf_op jit(solution)/shard_map/gather | solution.py:112
  207.5 2.9 %reshape.92 = f32[384,2,512]{2,1,0:T(2,128)} reshape(bf16[768,512]{1,0:T(8,128)(2,1)} %gather_fusion.1) | data formatting | bytes 2359296 | tf_op jit(solution)/shard_map/convert_element_type | solution.py:113
  210.4 3.6 %multiply_reduce_fusion = f32[384,512]{1,0:T(8,128)S(1)} fusion(f32[384,2,512]{2,1,0:T(2,128)} %reshape.92, f32[384,2]{1,0:T(8,128)S(1)} %copy.20), kind=kLoop, calls=%fused_computation.14 | loop fusion | flops 589824 | bytes 2362368 | tf_op jit(solution)/shard_map/reduce_sum | solution.py:114
  214.0 3.4 %fusion.6 = bf16[384,512]{1,0:T(8,128)(2,1)} fusion(f32[384,512]{1,0:T(8,128)S(1)} %multiply_reduce_fusion, bf16[256,512]{1,0:T(8,128)(2,1)S(1)} %copy-done.8, bf16[384,2048]{1,0:T(8,128)(2,1)} %fusion.4, bf16[2048,256]{1,0:T(8,128)(2,1)} %param.28, f32[384,256]{1,0:T(8,128)} %fusion.75), kind=kOutput, calls=%fused_computation.16 | convolution fusion | flops 504299520 | bytes 4456448 | tf_op jit(solution)/shard_map/dot_general | solution.py:69
  (47 shorter events, 1.4 us)
Async XLA Ops:
  7.2 131.4 %copy-start = (bf16[512,2048]{1,0:T(8,128)(2,1)S(1)}, bf16[512,2048]{1,0:T(8,128)(2,1)}, u32[]{:S(2)}) copy-start(bf16[512,2048]{1,0:T(8,128)(2,1)} %param.19) | copy-start | bytes 6291460
  7.2 100.1 %all-gather.2.cloned.1.call-start = ((), (), s32[]{:S(2)}) async-start(), calls=%async_computation.5 | async-start | bytes 5898240 | tf_op jit(solution)/shard_map/all_gather | solution.py:94
  15.2 1.9 copy-start.1
  15.2 2.5 %copy-start.5 = (f32[2048]{0:T(1024)S(1)}, f32[2048]{0:T(1024)}, u32[]{:S(2)}) copy-start(f32[2048]{0:T(1024)} %param.21) | copy-start | bytes 24580
  34.7 72.5 %copy-start.7 = (bf16[1,2048,256]{2,1,0:T(8,128)(2,1)S(1)}, bf16[1,2048,256]{2,1,0:T(8,128)(2,1)}, u32[]{:S(2)}) copy-start(bf16[1,2048,256]{2,1,0:T(8,128)(2,1)} %param.24) | copy-start | bytes 3145732
  71.0 99.3 %reduce-scatter.5.cloned.1.call-start = ((), (), s32[]{:S(2)}) async-start(), calls=%async_computation.6 | async-start | bytes 5898240 | tf_op jit(solution)/shard_map/reduce_scatter | solution.py:105
  122.3 1.0 copy-start.2
  122.3 1.1 copy-start.3
  122.3 4.9 %copy-start.4 = (bf16[31,512]{1,0:T(8,128)(2,1)S(1)}, bf16[31,512]{1,0:T(8,128)(2,1)}, u32[]{:S(2)}) copy-start(bf16[31,512]{1,0:T(8,128)(2,1)} %param.17) | copy-start | bytes 95236
  122.3 95.2 %reduce-scatter.3.cloned.1.call-start = ((), (), s32[]{:S(2)}) async-start(), calls=%async_computation.4 | async-start | bytes 1966080 | tf_op jit(solution)/shard_map/reduce_scatter | solution.py:102
  123.6 5.0 %collective-permute-start = (bf16[30,512]{1,0:T(8,128)(2,1)S(1)}, bf16[30,512]{1,0:T(8,128)(2,1)S(1)}, u32[]{:S(2)}, u32[]{:S(2)}) collective-permute-start(bf16[30,512]{1,0:T(8,128)(2,1)S(1)} %slice.265), channel_id=1, source_target_pairs={{0,4},{4,8},{8,12},{12,16},{16,20},{20,24},{24,28},{1,5},{5,9},{9,... | collective-permute-start | bytes 92168 | tf_op jit(solution)/shard_map/ppermute | solution.py:12
  128.7 9.8 %copy-start.9 = (f32[512]{0:T(512)S(1)}, f32[512]{0:T(512)}, u32[]{:S(2)}) copy-start(f32[512]{0:T(512)} %param.18) | copy-start | bytes 6148
  140.9 34.9 %copy-start.6 = (f32[384,2]{0,1:T(2,128)S(1)}, f32[384,2]{0,1:T(2,128)}, u32[]{:S(2)}) copy-start(f32[384,2]{0,1:T(2,128)} %param.23) | copy-start | bytes 9220
  170.3 33.9 %all-to-all-start.1 = ((bf16[8,144,512]{2,1,0:T(8,128)(2,1)}), bf16[8,144,512]{2,1,0:T(8,128)(2,1)S(1)}, u32[]{:S(2)}, u32[]{:S(2)}) async-start(bf16[8,144,512]{2,1,0:T(8,128)(2,1)} %bitcast.65), calls=%async_computation.3 | async-start | bytes 2359296 | tf_op jit(solution)/shard_map/all_to_all | solution.py:111
  210.4 3.6 %copy-start.8 = (bf16[256,512]{1,0:T(8,128)(2,1)S(1)}, bf16[256,512]{1,0:T(8,128)(2,1)}, u32[]{:S(2)}) copy-start(bf16[256,512]{1,0:T(8,128)(2,1)} %param.29) | copy-start | bytes 786436
Sparse Core Ops, SparseCore 0:
  71.1 36.0 all-gather.1
  122.4 47.7 reduce-scatter.4
  173.4 28.0 reduce-scatter.2
where the time goes:
time: 225 us; the launch traced here: 224 us
  waiting for transfers between devices  92.1 us (41%)
  blocking collectives  42.2 us (19%)
  local copies, waits for them, and re-layouts  25.1 us (11%)
  matrix products  23.8 us (11%)
  other arithmetic  17.5 us (8%)
  between operations  14 us (6%)
  starting transfers between devices  9.2 us (4%)
    all_to_all x1, blocking collectives, local(): lax.all_to_all(column_block, 'ep', split_axis=0, concat_axis=0, tiled=True)  36.2 us
    all_gather x1, waiting for transfers between devices, local(): arrived = lax.all_gather(arrived, 'tp', axis=2, tiled=True)  36.2 us
    reduce_scatter x1, waiting for transfers between devices, local(): lax.psum_scatter(expert_partial.astype(jnp.bfloat16), 'tp', scatter_dimen...  29.3 us
    all_to_all x1, waiting for transfers between devices, local(): lax.all_to_all(expert_rows, 'ep', split_axis=0, concat_axis=0, tiled=True)  25.2 us
    gather x1, local copies, waits for them, and re-layouts, local(): normalized[token_index]  12.3 us
    dot_general x1, matrix products, local(): jnp.dot(hidden, expert_down[0], preferred_element_type=jnp.float32)  10.3 us
    psum x1, blocking collectives, local(): lax.psum((jnp.sum(convolved, axis=1), jnp.sum(convolved * convolved, axis...  5.96 us
    all_to_all x1, starting transfers between devices, local(): lax.all_to_all(expert_rows, 'ep', split_axis=0, concat_axis=0, tiled=True)  5.52 us
  transfers between devices with their start and end apart: 5, of which 4 were waited for; matrix products, arithmetic and copies ran while one was open for 10% of the time, Pallas kernels for 0%

commit v1 on v0

v1 whole, which is shorter than its diff:
```python
import functools

import jax
import jax.numpy as jnp
from jax import lax
from jax.experimental import pallas as pl
from jax.experimental.pallas import tpu as pltpu
from jax.sharding import PartitionSpec as P

epsilon = 1e-05
MESH = pl.DeviceIdType.MESH
f32 = jnp.float32
bf16 = jnp.bfloat16


def dot(a, b):
    return jnp.dot(a, b, preferred_element_type=f32)


def kernel(
    n, tp, cap,
    tok, gain, routes_t, weights_t, act,
    gate_h, up_h, down_h, sg_h, su_h, sd_h, proj_h,
    conv_out, moe_out,
    gate, up, down, sg, su, sd, proj,
    norm, rank_s, wt_s, out_buf, arr, p_send, p_own, p_recv, q_send, q_recv, fin, ret,
    shared, c_send, c_own, c_recv, cq_send, cq_recv,
    load_sem, a2a_s, a2a_r, fc_s, fc_r, fx_s, fx_r, f2_s, f2_r,
    p_s, p_r, q_s, q_r, ret_s, ret_r, c_sem,
):
    i = lax.axis_index("ep")
    j = lax.axis_index("tp")
    jx, jc = lax.div(j, 2), lax.rem(j, 2)
    partner = jx * 2 + 1 - jc
    across = (1 - jx) * 2 + jc
    rows, width = tok.shape
    quarter = width // tp

    barrier = pltpu.get_barrier_semaphore()

    def greet(d, _):
        pl.semaphore_signal(
            barrier, inc=1, device_id=(lax.rem(i + d, n), j), device_id_type=MESH
        )
        return 0

    lax.fori_loop(1, n, greet, 0)
    for t in (partner, across):
        pl.semaphore_signal(barrier, inc=1, device_id=(i, t), device_id_type=MESH)

    loads = [
        pltpu.make_async_copy(src, dst, load_sem.at[k])
        for k, (src, dst) in enumerate(
            ((proj_h, proj), (gate_h.at[0], gate), (up_h.at[0], up), (down_h.at[0], down),
             (sg_h, sg), (su_h, su), (sd_h, sd))
        )
    ]
    for load in loads:
        load.start()

    def columns(block):
        return pl.ds(pl.multiple_of(block * quarter, quarter), quarter)

    experts = rank_s.shape[0]
    e_iota = lax.broadcasted_iota(jnp.int32, (experts, rows), 0)
    chosen = jnp.zeros((experts, rows), f32)
    weight = jnp.zeros((experts, rows), f32)
    for k in range(routes_t.shape[0]):
        hit = routes_t[k : k + 1, :] == e_iota
        chosen = jnp.where(hit, 1.0, chosen)
        weight = jnp.where(hit, weights_t[k : k + 1, :], weight)
    earlier = (
        lax.broadcasted_iota(jnp.int32, (rows, rows), 0)
        < lax.broadcasted_iota(jnp.int32, (rows, rows), 1)
    )
    rank = dot(chosen.astype(bf16), jnp.where(earlier, 1.0, 0.0).astype(bf16))
    rank_s[...] = jnp.where(chosen > 0.0, rank, -1.0).astype(jnp.int32)
    wt_s[...] = weight

    piece = rows // 8

    def norm_rows(r, _):
        at = pl.ds(pl.multiple_of(r * piece, piece), piece)
        x = tok[at, :].astype(f32)
        c = x - jnp.mean(x, axis=1, keepdims=True)
        v = jnp.mean(c * c, axis=1, keepdims=True)
        norm[at, :] = (c * lax.rsqrt(v + epsilon) * gain[...]).astype(bf16)
        return 0

    lax.fori_loop(0, 8, norm_rows, 0)

    slot = lax.broadcasted_iota(jnp.int32, (cap, rows), 0)

    def pick(e):
        return slot == rank_s[pl.ds(e, 1), :]

    def fill(d, _):
        e = lax.rem(i + d, n)
        chosen_rows = jnp.where(pick(e), 1.0, 0.0).astype(bf16)
        out_buf[e] = dot(chosen_rows, norm[:, columns(j)]).astype(bf16)
        return 0

    lax.fori_loop(1, n, fill, 0)
    pl.semaphore_wait(barrier, n + 1)

    def to_expert(e):
        return pltpu.make_async_remote_copy(
            src_ref=out_buf.at[e], dst_ref=arr.at[j, i], send_sem=a2a_s.at[e],
            recv_sem=a2a_r.at[i], device_id=(e, j), device_id_type=MESH,
        )

    def from_source(s):
        return pltpu.make_async_remote_copy(
            src_ref=out_buf.at[s], dst_ref=arr.at[j, s], send_sem=a2a_s.at[s],
            recv_sem=a2a_r.at[s], device_id=(s, j), device_id_type=MESH,
        )

    def send(d, _):
        to_expert(lax.rem(i + d, n)).start()
        return 0

    lax.fori_loop(1, n, send, 0)

    def forward(block, s, to, ss, rs):
        return pltpu.make_async_remote_copy(
            src_ref=arr.at[block, s], dst_ref=arr.at[block, s], send_sem=ss.at[s],
            recv_sem=rs.at[s], device_id=(i, to), device_id_type=MESH,
        )

    def move(src, dst, ss, rs, ep_at, tp_at):
        return pltpu.make_async_remote_copy(
            src_ref=src, dst_ref=dst, send_sem=ss, recv_sem=rs,
            device_id=(ep_at, tp_at), device_id_type=MESH,
        )

    loads[0].wait()
    for half in range(2):
        c_send[half] = dot(act[...], proj[:, columns(half * 2 + 1 - jc)]).astype(bf16)
    c_one = move(c_send, c_recv, c_sem.at[0], c_sem.at[1], i, partner)
    c_one.start()
    for half in range(2):
        c_own[half] = dot(act[...], proj[:, columns(half * 2 + jc)]).astype(bf16)
    own_rows = jnp.where(pick(i), 1.0, 0.0).astype(bf16)
    for block in range(tp):
        arr[block, i] = dot(
            own_rows, norm[:, block * quarter : (block + 1) * quarter]
        ).astype(bf16)
    c_one.wait()
    cq_send[...] = (c_own[1 - jx].astype(f32) + c_recv[1 - jx].astype(f32)).astype(bf16)
    c_two = move(cq_send, cq_recv, c_sem.at[2], c_sem.at[3], i, across)
    c_two.start()

    for load in loads[4:]:
        load.wait()
    shared_hidden = (
        jax.nn.silu(dot(norm[...], sg[...])) * dot(norm[...], su[...])
    ).astype(bf16)
    shared[...] = dot(shared_hidden, sd[...])
    for load in loads[1:4]:
        load.wait()

    def p_copy(s):
        return move(p_send.at[s], p_recv.at[s], p_s.at[s], p_r.at[s], i, partner)

    def q_copy(s):
        return move(q_send.at[s], q_recv.at[s], q_s.at[s], q_r.at[s], i, across)

    def back_to(s):
        return move(fin.at[s], ret.at[i], ret_s.at[s], ret_r.at[i], s, j)

    def back_from(e):
        return move(fin.at[e], ret.at[e], ret_s.at[e], ret_r.at[e], e, j)

    block_x = across
    block_2 = (1 - jx) * 2 + 1 - jc

    def step(d, _):
        s0 = lax.rem(i - d + 2 * n, n)
        s1 = lax.rem(i - d + 1 + 2 * n, n)
        s2 = lax.rem(i - d + 2 + 2 * n, n)
        s3 = lax.rem(i - d + 3 + 2 * n, n)
        s4 = lax.rem(i - d + 4 + 2 * n, n)

        @pl.when(d < n)
        def _():
            from_source(s0).wait_recv()
            forward(j, s0, across, fx_s, fx_r).start()
            forward(j, s0, partner, fc_s, fc_r).start()

        @pl.when((d >= 2) & (d - 1 < n))
        def _():
            forward(block_x, s1, across, fx_s, fx_r).wait_recv()
            forward(block_x, s1, partner, f2_s, f2_r).start()

        @pl.when((d >= 3) & (d - 2 < n))
        def _():
            forward(partner, s2, partner, fc_s, fc_r).wait_recv()
            forward(block_2, s2, partner, f2_s, f2_r).wait_recv()

        @pl.when((d >= 2) & (d - 2 < n))
        def _():
            g = jnp.zeros((cap, gate.shape[1]), f32)
            u = jnp.zeros((cap, gate.shape[1]), f32)
            for block in range(tp):
                x = arr[block, s2]
                at = slice(block * quarter, (block + 1) * quarter)
                g = g + dot(x, gate[at, :])
                u = u + dot(x, up[at, :])
            hidden = (jax.nn.silu(g) * u).astype(bf16)
            for half in range(2):
                p_send[s2, half] = dot(hidden, down[:, columns(half * 2 + 1 - jc)]).astype(bf16)
            for half in range(2):
                p_own[s2, half] = dot(hidden, down[:, columns(half * 2 + jc)]).astype(bf16)
            p_copy(s2).start()

        @pl.when((d >= 3) & (d - 3 < n))
        def _():
            p_copy(s3).wait_recv()
            q_send[s3] = (
                p_own[s3, 1 - jx].astype(f32) + p_recv[s3, 1 - jx].astype(f32)
            ).astype(bf16)
            q_copy(s3).start()

        @pl.when((d >= 4) & (d - 4 < n))
        def _():
            q_copy(s4).wait_recv()
            total = (
                p_own[s4, jx].astype(f32) + p_recv[s4, jx].astype(f32) + q_recv[s4].astype(f32)
            ).astype(bf16)

            @pl.when(d == 4)
            def _():
                ret[i] = total

            @pl.when(d > 4)
            def _():
                fin[s4] = total
                back_to(s4).start()

        return 0

    lax.fori_loop(1, n + 4, step, 0)

    c_two.wait()
    conv_out[...] = (
        c_own[jx].astype(f32) + c_recv[jx].astype(f32) + cq_recv[...].astype(f32)
    ).astype(bf16)

    def combine(e):
        hit = pick(e)
        w = wt_s[pl.ds(e, 1), :]
        high = w.astype(bf16).astype(f32)
        low = w - high
        rows_back = ret[e]
        total = jnp.zeros(shared.shape, f32)
        for part in (high, low):
            m = jnp.where(hit, part, 0.0).astype(bf16)
            total = total + lax.dot_general(
                m, rows_back, (((0,), (0,)), ((), ())), preferred_element_type=f32
            )
        shared[...] += total

    combine(i)

    def gather(d, _):
        e = lax.rem(i + d, n)
        back_from(e).wait_recv()
        combine(e)
        return 0

    lax.fori_loop(1, n, gather, 0)
    moe_out[...] = shared[...].astype(bf16)

    def drain(d, _):
        s = lax.rem(i + d, n)
        to_expert(s).wait_send()
        forward(j, s, across, fx_s, fx_r).wait_send()
        forward(j, s, partner, fc_s, fc_r).wait_send()
        forward(block_x, s, partner, f2_s, f2_r).wait_send()
        back_to(s).wait_send()
        return 0

    lax.fori_loop(1, n, drain, 0)

    def drain_all(s, _):
        p_copy(s).wait_send()
        q_copy(s).wait_send()
        return 0

    lax.fori_loop(0, n, drain_all, 0)


def conv_rows(conv_value, conv_gate, conv_taps, conv_gain, model_width):
    tok_rows = conv_value.shape[0]
    taps = conv_taps.shape[0]
    gated_rows = (
        conv_value.astype(f32) * jax.nn.sigmoid(conv_gate.astype(f32))
    ).astype(bf16)
    devices = lax.axis_size("ep")
    previous = lax.ppermute(
        gated_rows[tok_rows - (taps - 1) :], "ep", [(i, i + 1) for i in range(devices - 1)]
    )
    padded = jnp.concatenate([previous, gated_rows], axis=0).astype(f32)
    tap_weights = conv_taps.astype(f32)
    convolved = jnp.zeros(gated_rows.shape, f32)
    for offset in range(taps):
        convolved = convolved + tap_weights[offset][None, :] * padded[offset : offset + tok_rows]
    total_sum, square_sum = lax.psum(
        (jnp.sum(convolved, axis=1), jnp.sum(convolved * convolved, axis=1)), "tp"
    )
    average = total_sum / model_width
    variance = square_sum / model_width - average * average
    scaled = (
        (convolved - average[:, None]) * lax.rsqrt(variance + epsilon)[:, None] * conv_gain[None, :]
    )
    return jax.nn.silu(scaled).astype(bf16)


def local(
    conv_value, conv_gate, conv_taps, conv_gain, conv_proj, moe_tokens, moe_gain, routes,
    route_weights, expert_gate, expert_up, expert_down, shared_gate, shared_up, shared_down,
):
    n, tp = lax.axis_size("ep"), lax.axis_size("tp")
    assert tp == 4
    rows, width = moe_tokens.shape
    quarter = width // tp
    cap = 3 * rows * routes.shape[1] // (2 * n)
    cap = -(-cap // 16) * 16
    ff = expert_gate.shape[2]
    activated = conv_rows(conv_value, conv_gate, conv_taps, conv_gain, width)
    vmem = pl.BlockSpec(memory_space=pltpu.VMEM)
    anywhere = pl.BlockSpec(memory_space=pl.ANY)
    V = pltpu.VMEM
    dma = pltpu.SemaphoreType.DMA
    return pl.pallas_call(
        functools.partial(kernel, n, tp, cap),
        out_shape=(
            jax.ShapeDtypeStruct((rows, quarter), bf16),
            jax.ShapeDtypeStruct((rows, quarter), bf16),
        ),
        in_specs=[vmem] * 5 + [anywhere] * 7,
        out_specs=(vmem, vmem),
        scratch_shapes=[
            V((width, ff), bf16), V((width, ff), bf16), V((ff, width), bf16),
            V(shared_gate.shape, bf16), V(shared_up.shape, bf16), V(shared_down.shape, bf16),
            V(conv_proj.shape, bf16),
            V((rows, width), bf16), V((n, rows), jnp.int32), V((n, rows), f32),
            V((n, cap, quarter), bf16), V((tp, n, cap, quarter), bf16),
            V((n, 2, cap, quarter), bf16), V((n, 2, cap, quarter), bf16),
            V((n, 2, cap, quarter), bf16),
            V((n, cap, quarter), bf16), V((n, cap, quarter), bf16),
            V((n, cap, quarter), bf16), V((n, cap, quarter), bf16),
            V((rows, quarter), f32),
            V((2, rows, quarter), bf16), V((2, rows, quarter), bf16), V((2, rows, quarter), bf16),
            V((rows, quarter), bf16), V((rows, quarter), bf16),
            dma((7,)),
        ] + [dma((n,))] * 14 + [dma((4,))],
        compiler_params=pltpu.CompilerParams(
            collective_id=0, has_side_effects=True, vmem_limit_bytes=60 * 1024 * 1024
        ),
    )(
        moe_tokens, moe_gain[None, :], routes.T, route_weights.T, activated,
        expert_gate, expert_up, expert_down, shared_gate, shared_up, shared_down, conv_proj,
    )


def solution(mesh):
    placed = (
        P("ep", "tp"),
        P("ep", "tp"),
        P(None, "tp"),
        P("tp"),
        P("tp", None),
        P("ep", None),
        P(),
        P("ep", None),
        P("ep", None),
        P("ep", None, "tp"),
        P("ep", None, "tp"),
        P("ep", "tp", None),
        P(),
        P(),
        P(None, "tp"),
    )
    return jax.shard_map(
        local, mesh=mesh, in_specs=placed, out_specs=(P("ep", "tp"), P("ep", "tp")), check_vma=False
    )
```

time: 225 us -> 110 us (0.49)
  waiting for transfers between devices: 92.1 us -> 0.01 us
  Pallas kernels: 0 us -> 85.3 us
  blocking collectives: 42.2 us -> 6.31 us
  matrix products: 23.8 us -> 0 us
  local copies, waits for them, and re-layouts: 25.1 us -> 5.62 us
  between operations: 14 us -> 0.7 us
  other arithmetic: 17.5 us -> 6.36 us
  starting transfers between devices: 9.2 us -> 4.9 us
    pallas_call x0 -> x1, Pallas kernels: none -> 85.3 us  [local(): pl.pallas_call(functools.partial(kernel, n, tp, cap), out_shape=(jax.Shap...]
    all_to_all x1 -> x0, blocking collectives: 36.2 us -> none  [local(): lax.all_to_all(column_block, 'ep', split_axis=0, concat_axis=0, tiled=True)]
    all_gather x1 -> x0, waiting for transfers between devices: 36.2 us -> none  [local(): arrived = lax.all_gather(arrived, 'tp', axis=2, tiled=True)]
    reduce_scatter x2 -> x0, waiting for transfers between devices: 29.3 us -> none  [the longest x1 29.3 us: local(): lax.psum_scatter(expert_partial.astype(jnp.bfloat16), 'tp', scatter_dimen...]
    all_to_all x1 -> x0, waiting for transfers between devices: 25.2 us -> none  [local(): lax.all_to_all(expert_rows, 'ep', split_axis=0, concat_axis=0, tiled=True)]
    dot_general x5 -> x0, matrix products: 23.8 us -> none  [the longest x1 10.3 us: local(): jnp.dot(hidden, expert_down[0], preferred_element_type=jnp.float32)]
    gather x2 -> x0, local copies, waits for them, and re-layouts: 15.6 us -> none  [the longest x1 12.3 us: local(): normalized[token_index]]
    reduce_sum x5 -> x1, other arithmetic: 9.87 us -> 3.83 us  [conv_rows(): jnp.sum(convolved, axis=1)]
  transfers between devices with their start and end apart: 5 -> 1, of which waited for: 4 -> 0; matrix products, arithmetic and copies ran while one was open for 10% -> 2% of each run, Pallas kernels for 0% -> 0%
where the time goes in v1:
time: 110 us; the launch traced here: 109 us
  Pallas kernels  85.3 us (78%)
  other arithmetic  6.36 us (6%)
  blocking collectives  6.31 us (6%)
  local copies, waits for them, and re-layouts  5.62 us (5%)
  starting transfers between devices  4.9 us (4%)
    pallas_call x1, Pallas kernels, local(): pl.pallas_call(functools.partial(kernel, n, tp, cap), out_shape=(jax.Shap...  85.3 us
    psum x1, blocking collectives, conv_rows(): lax.psum((jnp.sum(convolved, axis=1), jnp.sum(convolved * convolved, axis...  6.31 us
    ppermute x1, starting transfers between devices, conv_rows(): lax.ppermute(gated_rows[tok_rows - (taps - 1):], 'ep', [(i, i + 1) for i...  4.9 us
    reduce_sum x1, other arithmetic, conv_rows(): jnp.sum(convolved, axis=1)  3.83 us
    unnamed x4, local copies, waits for them, and re-layouts  3.54 us
  transfers between devices with their start and end apart: 1, of which 0 were waited for; matrix products, arithmetic and copies ran while one was open for 2% of the time, Pallas kernels for 0%

profile of v1, /device:TPU:0, one launch (start us, length us, event | category | flops | bytes accessed | tf_op | source)
XLA Modules:
  0.0 109.1 jit_solution(17060375396225749800)
XLA Ops:
  0.6 1.3 %multiply_convert_fusion.1 = bf16[384,512]{1,0:T(8,128)(2,1)S(1)} fusion(bf16[384,512]{1,0:T(8,128)(2,1)} %param.16, bf16[384,512]{1,0:T(8,128)(2,1)} %param.15), kind=kLoop, calls=%fused_computation.63 | loop fusion | flops 1376256 | bytes 1179648 | tf_op jit(solution)/shard_map/convert_element_type | solution.py:298
  2.0 4.9 %collective-permute-start = (bf16[30,512]{1,0:T(8,128)(2,1)S(1)}, bf16[30,512]{1,0:T(8,128)(2,1)S(1)}, u32[]{:S(2)}, u32[]{:S(2)}) collective-permute-start(bf16[30,512]{1,0:T(8,128)(2,1)S(1)} %slice.253), channel_id=1, source_target_pairs={{0,4},{4,8},{8,12},{12,16},{16,20},{20,24},{24,28},{1,5},{5,9},{9,... | collective-permute-start | bytes 92168 | tf_op jit(solution)/shard_map/ppermute | solution.py:300
  6.9 1.1 fusion.32
  8.0 1.0 fusion.33
  9.0 0.0 collective-permute-done
  9.0 0.1 maximum_convert_fusion
  9.1 0.0 copy-start
  9.1 3.8 %fusion.30 = (f32[384]{0:T(512)S(1)}, f32[384]{0:T(512)S(1)}, f32[384,512]{1,0:T(8,128)S(1)}) fusion(f32[414,512]{1,0:T(8,128)S(1)} %maximum_convert_fusion, f32[512]{0:T(512)S(1)} %bitcast.64, f32[512]{0:T(512)S(1)} %bitcast.63, f32[512]{0:T(512)S(1)} %bitcast.62, f32[512]{0:T(512)S(1)} %bitcast.61, f32[512]{0:T(512)S(1)} %bitcast.60, f32[512]{0:T(512)S(1)} %bitcast.59, ...), kind=kLoop, calls=%fused_computation.67 | loop fusion | flops 12582144 | bytes 25232384 | tf_op jit(solution)/shard_map/reduce_sum | solution.py:309
  13.0 6.3 %all-reduce = (f32[384]{0:T(512)S(1)}, f32[384]{0:T(512)S(1)}) all-reduce(f32[384]{0:T(512)S(1)} %get-tuple-element.3, f32[384]{0:T(512)S(1)} %get-tuple-element.2), channel_id=1, replica_groups=mesh['ep'=8,'tp'=4] {'tp'}, use_global_device_ids=true, to_apply=%region_3.0 | all-reduce | flops 768 | bytes 6144 | tf_op jit(solution)/shard_map/psum | solution.py:308
  19.3 0.0 copy-done
  19.3 1.1 multiply_convert_fusion.act
  20.3 85.3 %shard_map.158 = (bf16[384,512]{1,0:T(8,128)(2,1)}, bf16[384,512]{1,0:T(8,128)(2,1)}) custom-call(bf16[384,2048]{1,0:T(8,128)(2,1)} %tok.1, f32[1,2048]{1,0:T(1,128)} %bitcast.65, s32[2,384]{1,0:T(2,128)} %bitcast.66, f32[2,384]{1,0:T(2,128)} %bitcast.67, bf16[384,512]{1,0:T(8,128)(2,1)} %multiply_convert_fusion.act, bf16[1,2048,256]{2,1,0:T(8,128)(2,1)} %gate_h.1, ...), custom_call_target="tpu_custom_call" | custom-call | tf_op jit(solution)/shard_map/pallas_call | solution.py:335
  105.6 1.8 %copy.19 = bf16[384,512]{1,0:T(8,128)(2,1)} copy(bf16[384,512]{1,0:T(8,128)(2,1)} %get-tuple-element.42) | data formatting | bytes 786432
  107.4 1.8 %copy.20 = bf16[384,512]{1,0:T(8,128)(2,1)} copy(bf16[384,512]{1,0:T(8,128)(2,1)} %get-tuple-element.43) | data formatting | bytes 786432
  (2 shorter events, 0.0 us)
Async XLA Ops:
  2.0 7.0 %collective-permute-start = (bf16[30,512]{1,0:T(8,128)(2,1)S(1)}, bf16[30,512]{1,0:T(8,128)(2,1)S(1)}, u32[]{:S(2)}, u32[]{:S(2)}) collective-permute-start(bf16[30,512]{1,0:T(8,128)(2,1)S(1)} %slice.253), channel_id=1, source_target_pairs={{0,4},{4,8},{8,12},{12,16},{16,20},{20,24},{24,28},{1,5},{5,9},{9,... | collective-permute-start | bytes 92168 | tf_op jit(solution)/shard_map/ppermute | solution.py:300
  9.1 10.2 %copy-start = (f32[512]{0:T(512)S(1)}, f32[512]{0:T(512)}, u32[]{:S(2)}) copy-start(f32[512]{0:T(512)} %param.18) | copy-start | bytes 6148

commit v2 on v1

--- a/solution.py
+++ b/solution.py
@@ -19,14 +19,15 @@
 
 def kernel(
     n, tp, cap,
-    tok, gain, routes_t, weights_t, act,
+    tok, gain, routes_t, weights_t, conv_gain, value_h, cgate_h, taps_h,
     gate_h, up_h, down_h, sg_h, su_h, sd_h, proj_h,
     conv_out, moe_out,
     gate, up, down, sg, su, sd, proj,
     norm, rank_s, wt_s, out_buf, arr, p_send, p_own, p_recv, q_send, q_recv, fin, ret,
+    value, cgate, taps, pad, halo_out, halo_in, conv, stats, stat_a, stat_b, stat_c, stat_d,
     shared, c_send, c_own, c_recv, cq_send, cq_recv,
     load_sem, a2a_s, a2a_r, fc_s, fc_r, fx_s, fx_r, f2_s, f2_r,
-    p_s, p_r, q_s, q_r, ret_s, ret_r, c_sem,
+    p_s, p_r, q_s, q_r, ret_s, ret_r, c_sem, h_sem,
 ):
     i = lax.axis_index("ep")
     j = lax.axis_index("tp")
@@ -52,7 +53,8 @@
         pltpu.make_async_copy(src, dst, load_sem.at[k])
         for k, (src, dst) in enumerate(
             ((proj_h, proj), (gate_h.at[0], gate), (up_h.at[0], up), (down_h.at[0], down),
-             (sg_h, sg), (su_h, su), (sd_h, sd))
+             (sg_h, sg), (su_h, su), (sd_h, sd), (value_h, value), (cgate_h, cgate),
+             (taps_h, taps))
         )
     ]
     for load in loads:
@@ -101,7 +103,24 @@
         return 0
 
     lax.fori_loop(1, n, fill, 0)
+
+    for load in loads[7:]:
+        load.wait()
+    lead = halo_out.shape[0]
+    gated = (value[...].astype(f32) * jax.nn.sigmoid(cgate[...].astype(f32))).astype(bf16)
+    pad[lead:, :] = gated.astype(f32)
+    halo_out[...] = gated[rows - lead :, :]
     pl.semaphore_wait(barrier, n + 1)
+
+    def halo(ep_at):
+        return pltpu.make_async_remote_copy(
+            src_ref=halo_out, dst_ref=halo_in, send_sem=h_sem.at[0], recv_sem=h_sem.at[1],
+            device_id=(ep_at, j), device_id_type=MESH,
+        )
+
+    @pl.when(i < n - 1)
+    def _():
+        halo(i + 1).start()
 
     def to_expert(e):
         return pltpu.make_async_remote_copy(
@@ -133,31 +152,71 @@
             device_id=(ep_at, tp_at), device_id_type=MESH,
         )
 
-    loads[0].wait()
-    for half in range(2):
-        c_send[half] = dot(act[...], proj[:, columns(half * 2 + 1 - jc)]).astype(bf16)
-    c_one = move(c_send, c_recv, c_sem.at[0], c_sem.at[1], i, partner)
-    c_one.start()
-    for half in range(2):
-        c_own[half] = dot(act[...], proj[:, columns(half * 2 + jc)]).astype(bf16)
     own_rows = jnp.where(pick(i), 1.0, 0.0).astype(bf16)
     for block in range(tp):
         arr[block, i] = dot(
             own_rows, norm[:, block * quarter : (block + 1) * quarter]
         ).astype(bf16)
-    c_one.wait()
-    cq_send[...] = (c_own[1 - jx].astype(f32) + c_recv[1 - jx].astype(f32)).astype(bf16)
-    c_two = move(cq_send, cq_recv, c_sem.at[2], c_sem.at[3], i, across)
-    c_two.start()
-
-    for load in loads[4:]:
+    for load in loads[:7]:
         load.wait()
-    shared_hidden = (
-        jax.nn.silu(dot(norm[...], sg[...])) * dot(norm[...], su[...])
-    ).astype(bf16)
-    shared[...] = dot(shared_hidden, sd[...])
-    for load in loads[1:4]:
-        load.wait()
+
+    @pl.when(i == 0)
+    def _():
+        pad[:lead, :] = jnp.zeros((lead, quarter), f32)
+
+    @pl.when(i > 0)
+    def _():
+        halo(i - 1).wait_recv()
+        pad[:lead, :] = halo_in[...].astype(f32)
+
+    taken = rows // 4
+    lanes = 128
+
+    def conv_piece(q):
+        first = pl.multiple_of(q * taken, taken)
+        weights = taps[...].astype(f32)
+        skip = lead - (taps.shape[0] - 1)
+        sums = jnp.zeros((taken, 1), f32)
+        squares = jnp.zeros((taken, 1), f32)
+        for c in range(quarter // lanes):
+            at = slice(c * lanes, (c + 1) * lanes)
+            window = pad[pl.ds(first, taken + lead), at]
+            total = jnp.zeros((taken, lanes), f32)
+            for low in range(8):
+                turned = window if low == 0 else pltpu.roll(window, taken + lead - low, 0)
+                for tap in range(taps.shape[0]):
+                    if (skip + tap) % 8 == low:
+                        begin = skip + tap - low
+                        total = total + weights[tap : tap + 1, at] * turned[begin : begin + taken]
+            conv[pl.ds(first, taken), at] = total
+            sums = sums + jnp.sum(total, axis=1, keepdims=True)
+            squares = squares + jnp.sum(total * total, axis=1, keepdims=True)
+        lane = lax.broadcasted_iota(jnp.int32, (taken, lanes), 1)
+        stats[pl.ds(first, taken), :] = jnp.where(lane == 0, sums, squares)
+
+    def stat_one():
+        return move(stat_a, stat_b, c_sem.at[4], c_sem.at[5], i, partner)
+
+    def stat_two():
+        return move(stat_c, stat_d, c_sem.at[6], c_sem.at[7], i, across)
+
+    def c_one():
+        return move(c_send, c_recv, c_sem.at[0], c_sem.at[1], i, partner)
+
+    def c_two():
+        return move(cq_send, cq_recv, c_sem.at[2], c_sem.at[3], i, across)
+
+    def conv_product():
+        both = stat_c[...] + stat_d[...]
+        spread = jnp.concatenate([both] * (lanes // 8), axis=0).T
+        average = spread[:, 0:1] / width
+        variance = spread[:, 1:2] / width - average * average
+        scaled = (conv[...] - average) * lax.rsqrt(variance + epsilon) * conv_gain[...]
+        act = jax.nn.silu(scaled).astype(bf16)
+        for half in range(2):
+            c_send[half] = dot(act, proj[:, columns(half * 2 + 1 - jc)]).astype(bf16)
+        for half in range(2):
+            c_own[half] = dot(act, proj[:, columns(half * 2 + jc)]).astype(bf16)
 
     def p_copy(s):
         return move(p_send.at[s], p_recv.at[s], p_s.at[s], p_r.at[s], i, partner)
@@ -237,11 +296,47 @@
                 fin[s4] = total
                 back_to(s4).start()
 
+        @pl.when(d <= 4)
+        def _():
+            conv_piece(d - 1)
+
+        @pl.when(d == 4)
+        def _():
+            stat_a[...] = stats[...].T[:8, :]
+            stat_one().start()
+
+        @pl.when(d == 5)
+        def _():
+            stat_one().wait()
+            stat_c[...] = stat_a[...] + stat_b[...]
+            stat_two().start()
+
+        @pl.when(d == 6)
+        def _():
+            stat_two().wait()
+            conv_product()
+            c_one().start()
+
+        @pl.when(d == 7)
+        def _():
+            c_one().wait()
+            cq_send[...] = (
+                c_own[1 - jx].astype(f32) + c_recv[1 - jx].astype(f32)
+            ).astype(bf16)
+            c_two().start()
+
+        @pl.when(d == 8)
+        def _():
+            shared_hidden = (
+                jax.nn.silu(dot(norm[...], sg[...])) * dot(norm[...], su[...])
+            ).astype(bf16)
+            shared[...] = dot(shared_hidden, sd[...])
+
         return 0
 
     lax.fori_loop(1, n + 4, step, 0)
 
-    c_two.wait()
+    c_two().wait()
     conv_out[...] = (
         c_own[jx].astype(f32) + c_recv[jx].astype(f32) + cq_recv[...].astype(f32)
     ).astype(bf16)
@@ -271,6 +366,10 @@
     lax.fori_loop(1, n, gather, 0)
     moe_out[...] = shared[...].astype(bf16)
 
+    @pl.when(i < n - 1)
+    def _():
+        halo(i + 1).wait_send()
+
     def drain(d, _):
         s = lax.rem(i + d, n)
         to_expert(s).wait_send()
@@ -288,32 +387,6 @@
         return 0
 
     lax.fori_loop(0, n, drain_all, 0)
-
-
-def conv_rows(conv_value, conv_gate, conv_taps, conv_gain, model_width):
-    tok_rows = conv_value.shape[0]
-    taps = conv_taps.shape[0]
-    gated_rows = (
-        conv_value.astype(f32) * jax.nn.sigmoid(conv_gate.astype(f32))
-    ).astype(bf16)
-    devices = lax.axis_size("ep")
-    previous = lax.ppermute(
-        gated_rows[tok_rows - (taps - 1) :], "ep", [(i, i + 1) for i in range(devices - 1)]
-    )
-    padded = jnp.concatenate([previous, gated_rows], axis=0).astype(f32)
-    tap_weights = conv_taps.astype(f32)
-    convolved = jnp.zeros(gated_rows.shape, f32)
-    for offset in range(taps):
-        convolved = convolved + tap_weights[offset][None, :] * padded[offset : offset + tok_rows]
-    total_sum, square_sum = lax.psum(
-        (jnp.sum(convolved, axis=1), jnp.sum(convolved * convolved, axis=1)), "tp"
-    )
-    average = total_sum / model_width
-    variance = square_sum / model_width - average * average
-    scaled = (
-        (convolved - average[:, None]) * lax.rsqrt(variance + epsilon)[:, None] * conv_gain[None, :]
-    )
-    return jax.nn.silu(scaled).astype(bf16)
 
 
 def local(
@@ -327,7 +400,7 @@
     cap = 3 * rows * routes.shape[1] // (2 * n)
     cap = -(-cap // 16) * 16
     ff = expert_gate.shape[2]
-    activated = conv_rows(conv_value, conv_gate, conv_taps, conv_gain, width)
+    lead = -(-(conv_taps.shape[0] - 1) // 16) * 16
     vmem = pl.BlockSpec(memory_space=pltpu.VMEM)
     anywhere = pl.BlockSpec(memory_space=pl.ANY)
     V = pltpu.VMEM
@@ -338,7 +411,7 @@
             jax.ShapeDtypeStruct((rows, quarter), bf16),
             jax.ShapeDtypeStruct((rows, quarter), bf16),
         ),
-        in_specs=[vmem] * 5 + [anywhere] * 7,
+        in_specs=[vmem] * 5 + [anywhere] * 10,
         out_specs=(vmem, vmem),
         scratch_shapes=[
             V((width, ff), bf16), V((width, ff), bf16), V((ff, width), bf16),
@@ -350,16 +423,21 @@
             V((n, 2, cap, quarter), bf16),
             V((n, cap, quarter), bf16), V((n, cap, quarter), bf16),
             V((n, cap, quarter), bf16), V((n, cap, quarter), bf16),
+            V((rows, quarter), bf16), V((rows, quarter), bf16), V(conv_taps.shape, bf16),
+            V((rows + lead, quarter), f32), V((lead, quarter), bf16), V((lead, quarter), bf16),
+            V((rows, quarter), f32), V((rows, 128), f32),
+            V((8, rows), f32), V((8, rows), f32), V((8, rows), f32), V((8, rows), f32),
             V((rows, quarter), f32),
             V((2, rows, quarter), bf16), V((2, rows, quarter), bf16), V((2, rows, quarter), bf16),
             V((rows, quarter), bf16), V((rows, quarter), bf16),
-            dma((7,)),
-        ] + [dma((n,))] * 14 + [dma((4,))],
+            dma((10,)),
+        ] + [dma((n,))] * 14 + [dma((8,)), dma((2,))],
         compiler_params=pltpu.CompilerParams(
             collective_id=0, has_side_effects=True, vmem_limit_bytes=60 * 1024 * 1024
         ),
     )(
-        moe_tokens, moe_gain[None, :], routes.T, route_weights.T, activated,
+        moe_tokens, moe_gain[None, :], routes.T, route_weights.T, conv_gain[None, :],
+        conv_value, conv_gate, conv_taps,
         expert_gate, expert_up, expert_down, shared_gate, shared_up, shared_down, conv_proj,
     )
 

time: 110 us -> 97.7 us (0.89)
  Pallas kernels: 85.3 us -> 93.3 us
  other arithmetic: 6.36 us -> 0 us
  blocking collectives: 6.31 us -> 0 us
  starting transfers between devices: 4.9 us -> 0 us
  local copies, waits for them, and re-layouts: 5.62 us -> 3.53 us
    pallas_call x1, Pallas kernels: 85.3 us -> 93.3 us  [local(): pl.pallas_call(functools.partial(kernel, n, tp, cap), out_shape=(jax.Shap...]
    psum x1 -> x0, blocking collectives: 6.31 us -> none  [conv_rows(): lax.psum((jnp.sum(convolved, axis=1), jnp.sum(convolved * convolved, axis...]
    ppermute x1 -> x0, starting transfers between devices: 4.9 us -> none  [conv_rows(): lax.ppermute(gated_rows[tok_rows - (taps - 1):], 'ep', [(i, i + 1) for i...]
    reduce_sum x1 -> x0, other arithmetic: 3.83 us -> none  [conv_rows(): jnp.sum(convolved, axis=1)]
    convert_element_type x3 -> x0, other arithmetic: 2.52 us -> none  [the longest x1 1.34 us: conv_rows(): gated_rows = (conv_value.astype(f32) * jax.nn.sigmoid(conv_gate.astype(f3...]
    slice x3 -> x0, local copies, waits for them, and re-layouts: 2.08 us -> none  [the longest x2 2.07 us: conv_rows(): tap_weights[offset][None, :] * padded[offset:offset + tok_rows]]
    unnamed x4 -> x2, local copies, waits for them, and re-layouts: 3.54 us -> 3.53 us
  transfers between devices with their start and end apart: 1 -> 0, of which waited for: 0 -> 0; matrix products, arithmetic and copies ran while one was open for 2% -> 0% of each run, Pallas kernels for 0% -> 0%
where the time goes in v2:
time: 97.7 us; the launch traced here: 97.4 us
  Pallas kernels  93.3 us (95%)
  local copies, waits for them, and re-layouts  3.53 us (4%)
    pallas_call x1, Pallas kernels, local(): pl.pallas_call(functools.partial(kernel, n, tp, cap), out_shape=(jax.Shap...  93.3 us
    unnamed x2, local copies, waits for them, and re-layouts  3.53 us

profile of v2, /device:TPU:0, one launch (start us, length us, event | category | flops | bytes accessed | tf_op | source)
XLA Modules:
  0.0 97.4 jit_solution(11825969040387631871)
XLA Ops:
  0.6 93.3 %shard_map.158 = (bf16[384,512]{1,0:T(8,128)(2,1)}, bf16[384,512]{1,0:T(8,128)(2,1)}) custom-call(bf16[384,2048]{1,0:T(8,128)(2,1)} %tok.1, f32[1,2048]{1,0:T(1,128)} %bitcast.4, s32[2,384]{1,0:T(2,128)} %bitcast.5, f32[2,384]{1,0:T(2,128)} %bitcast.6, f32[1,512]{1,0:T(1,128)} %bitcast.7, bf16[384,512]{1,0:T(8,128)(2,1)} %value_h.1, ...), custom_call_target="tpu_custom_call" | custom-call | tf_op jit(solution)/shard_map/pallas_call | solution.py:408
  93.9 1.8 %copy.19 = bf16[384,512]{1,0:T(8,128)(2,1)} copy(bf16[384,512]{1,0:T(8,128)(2,1)} %get-tuple-element.4) | data formatting | bytes 786432
  95.7 1.8 %copy.20 = bf16[384,512]{1,0:T(8,128)(2,1)} copy(bf16[384,512]{1,0:T(8,128)(2,1)} %get-tuple-element.5) | data formatting | bytes 786432
